TPU v7x, 32 devices: a whole 2x2x4 slice. The times are simulated.
32 devices in a mesh: grp: 2 (over x), sp: 4 (over y, core), tp: 4 (over z).
Axes of the slice: x: 2, y: 2, z: 4, core: 2. Of those that a mesh axis runs over, the one named last changes fastest.
Arguments:
- layer_input: bfloat16 [8, 1024, 2048], P(('grp', 'tp'), 'sp'), parts along dimension 0, may hold values from -6 to 6
- norm_gain: bfloat16 [2048], replicated, may hold values from 0.099609375 to 1.8984375
- key_weight: bfloat16 [2048, 1024], replicated, may hold values from -0.125 to 0.125
- value_weight: bfloat16 [2048, 1024], replicated, may hold values from -0.125 to 0.125
- input_gate_weight: bfloat16 [2048, 8], replicated, may hold values from -0.125 to 0.125
- forget_gate_weight: bfloat16 [2048, 8], replicated, may hold values from -0.125 to 0.125
- conv_weight: float32 [4, 1024], replicated, may hold values from -3 to 3
- input_shift: float32 [8, 8, 1024], P(('grp', 'sp'), 'tp'), parts along dimension 0, may hold values from -4 to 302
- forget_shift: float32 [8, 8, 1024], P(('grp', 'sp'), 'tp'), parts along dimension 0, may hold values from 0 to 10.1
- new_query: bfloat16 [8, 8, 128], P(('grp', 'sp'), 'tp'), parts along dimension 0, may hold values from 0.1 to 2
- new_key: bfloat16 [8, 8, 128], P(('grp', 'sp'), 'tp'), parts along dimension 0, may hold values from -6 to 6
- new_value: bfloat16 [8, 8, 128], P(('grp', 'sp'), 'tp'), parts along dimension 0, may hold values from -6 to 6
- new_input: float32 [8, 8], P(('grp', 'sp'), 'tp'), parts along dimension 0, may hold values from 2 to 6
- new_forget: float32 [8, 8], P(('grp', 'sp'), 'tp'), parts along dimension 0, may hold values from -1 to 3
Outputs:
- key_cache: bfloat16 [8, 8, 1024, 128], P(('grp', 'sp'), 'tp'), parts along dimension 0
- value_cache: bfloat16 [8, 8, 1024, 128], P(('grp', 'sp'), 'tp'), parts along dimension 0
- weight_cache: float32 [8, 8, 1024], P(('grp', 'sp'), 'tp'), parts along dimension 0
- first_read: bfloat16 [8, 8, 128], P(('grp', 'sp'), 'tp'), parts along dimension 0
There are 2 independent parts, one for each index of `grp`. A program takes and returns all parts, laid end to end along the dimension named above; an argument that names none is the same for every part. Nothing has to cross between parts.
All inputs are finite; a program needn't handle non-finite values.
Results may differ from a plain program's by a relative error of at most 0.012.
Values may be sent and summed in bfloat16 or wider, within the bound.
A program may use at most 64 MiB of HBM per device.

v0:
```python
import functools

import jax
import jax.numpy as jnp
from jax import lax
from jax.experimental import pallas as pl
from jax.experimental.pallas import tpu as pltpu
from jax.sharding import PartitionSpec as P

MESH = pl.DeviceIdType.MESH
epsilon = 1e-06
SPLIT = 2


def log_sigmoid(x):
    return jnp.minimum(x, 0.0) - jnp.log1p(jnp.exp(-jnp.abs(x)))


def kernel(
    dims,
    x_ref,
    gain_ref,
    wi_ref,
    wf_ref,
    conv_ref,
    ishift_ref,
    fshift_ref,
    query_ref,
    nkey_ref,
    nvalue_ref,
    ninput_ref,
    nforget_ref,
    wk_ref,
    wv_ref,
    keys_out,
    values_out,
    weight_out,
    read_out,
    wbuf,
    normed,
    comp,
    relay,
    final,
    gcomp,
    grelay,
    gfinal,
    ext,
    w_sem,
    s1_send,
    s1_recv,
    s2_send,
    f_recv,
):
    n, nsp, ns, nd, pos, heads, hl, dk, taps = dims
    chunks = [(kv, r) for kv in range(2) for r in range(SPLIT)]
    C = len(chunks)
    rows = pos // SPLIT
    length = nsp * pos
    t = lax.axis_index("tp")
    p = lax.axis_index("sp")
    high = (2 * t) // n
    direction = 1 - 2 * high
    targets = [lax.rem(t + direction * (1 + k) + n, n) for k in range(n)]

    barrier = pltpu.get_barrier_semaphore()
    for k in range(n - 1):
        pl.semaphore_signal(barrier, inc=1, device_id={"tp": targets[k]}, device_id_type=MESH)
    for k in range(nsp - 1):
        pl.semaphore_signal(
            barrier, inc=1, device_id={"sp": lax.rem(p + 1 + k, nsp)}, device_id_type=MESH
        )

    def weight_copy(k, kv):
        columns = pl.ds(pl.multiple_of(targets[k] * (hl * dk), dk), hl * dk)
        source = wv_ref if kv else wk_ref
        return pltpu.make_async_copy(source.at[:, columns], wbuf.at[k, kv], w_sem.at[k, kv])

    for k in range(n):
        for kv in range(2):
            weight_copy(k, kv).start()

    gain = gain_ref[...].astype(jnp.float32).reshape(1, -1)
    step = 32
    for i in range(ns):

        @pl.loop(0, pos // step)
        def _(at):
            window = pl.ds(pl.multiple_of(at * step, step), step)
            wide = x_ref[i, window, :].astype(jnp.float32)
            mean = jnp.mean(wide * wide, axis=-1, keepdims=True)
            normed[i, window, :] = (wide * lax.rsqrt(mean + epsilon) * gain).astype(jnp.bfloat16)

    def part(buf, lead, c):
        kv, r = chunks[c]
        return buf.at[(*lead, kv, slice(None), pl.ds(r * rows, rows), slice(None))]

    def s1_source(k, i, c):
        return gcomp.at[i] if c == C else part(comp, (k, i), c)

    def s1_target(b, i, c):
        return grelay.at[b, i] if c == C else part(relay, (b, i), c)

    def s1_copy(k, i, c):
        return pltpu.make_async_remote_copy(
            src_ref=s1_source(k, i, c),
            dst_ref=s1_target(t, i, c),
            send_sem=s1_send.at[k, i, c],
            recv_sem=s1_recv.at[t, i, c],
            device_id={"tp": targets[k]},
            device_id_type=MESH,
        )

    def f_target(d, at, c):
        if c == C:
            return gfinal.at[d, at]
        kv, r = chunks[c]
        window = pl.ds(pl.multiple_of(at * pos + r * rows, rows), rows)
        return (values_out if kv else final).at[d, :, window, :]

    def forward(k, b, i, c, begin):
        s = b * ns + i
        q = s // nd
        d = lax.rem(s, nd)
        source = s1_source(n - 1, i, c) if k == n - 1 else s1_target(b, i, c)
        remote = pltpu.make_async_remote_copy(
            src_ref=source,
            dst_ref=f_target(d, p, c),
            send_sem=s2_send.at[k, i, c],
            recv_sem=f_recv.at[d, p, c],
            device_id={"sp": q},
            device_id_type=MESH,
        )

        @pl.when(q != p)
        def _():
            if begin:
                remote.start()
            else:
                remote.wait_send()

        if begin:

            @pl.when(q == p)
            def _():
                pltpu.make_async_copy(source, f_target(d, p, c), f_recv.at[d, p, c]).start()

    def compute(k):
        for kv in range(2):
            weight_copy(k, kv).wait()
            for i in range(ns):
                y = jnp.dot(normed[i], wbuf[k, kv], preferred_element_type=jnp.float32)
                for h in range(hl):
                    comp[k, i, kv, h] = y[:, h * dk : (h + 1) * dk].astype(jnp.bfloat16)
            if k == 0 and kv == 0:
                pl.semaphore_wait(barrier, n - 1 + nsp - 1)
            for i in range(ns):
                for c in range(C):
                    if chunks[c][0] == kv:
                        if k == n - 1:
                            forward(k, t, i, c, True)
                        else:
                            s1_copy(k, i, c).start()

    def gates():
        for i in range(ns):
            for at, w in enumerate((wi_ref, wf_ref)):
                g = lax.dot_general(
                    w[...], normed[i], (((1,), (1,)), ((), ())), preferred_element_type=jnp.float32
                )
                gcomp[i, at * heads : (at + 1) * heads, :] = g.astype(jnp.bfloat16)
            for to in range(n - 1):
                s1_copy(to, i, C).start()
            forward(n - 1, t, i, C, True)

    for k in range(n):
        compute(k)
        if k == 0:
            gates()

    def origin(k):
        lower = k + (k >= t).astype(jnp.int32)
        upper = n - 1 - (k + (k >= n - 1 - t).astype(jnp.int32))
        return jnp.where(high == 0, lower, upper)

    def relay_step(k, c):
        b = origin(k)
        for i in range(ns):
            place = s1_target(b, i, c)
            pltpu.make_async_copy(place, place, s1_recv.at[b, i, c]).wait()
            forward(k, b, i, c, True)


    def arrived(d, at, c):
        place = f_target(d, at, c)
        pltpu.make_async_copy(place, place, f_recv.at[d, at, c]).wait()

    scaling = dk ** (-0.5)
    lane = lax.broadcasted_iota(jnp.int32, (8, length), 1)
    row = lax.broadcasted_iota(jnp.int32, (2 * heads, pos), 0)
    weights, fresh = {}, {}
    scores = {}

    def weigh():
        for d in range(nd):
            for at in range(nsp):
                arrived(d, at, C)
            for h in range(hl):

                def gate(base):
                    pieces = [
                        jnp.sum(
                            jnp.where(
                                row == base + t * hl + h, gfinal[d, at].astype(jnp.float32), 0.0
                            ),
                            axis=0,
                            keepdims=True,
                        )
                        for at in range(nsp)
                    ]
                    return jnp.concatenate(pieces, axis=1)

                log_forget = log_sigmoid(gate(heads) + fshift_ref[d, h : h + 1, :])
                suffix = pltpu.roll(jnp.broadcast_to(log_forget, (8, length)), length - 1, 1)
                suffix = jnp.where(lane < length - 1, suffix, 0.0)
                hop = 1
                while hop < length:
                    moved = pltpu.roll(suffix, length - hop, 1)
                    suffix = suffix + jnp.where(lane < length - hop, moved, 0.0)
                    hop *= 2
                new_input = ninput_ref[d : d + 1, h : h + 1]
                decay = log_sigmoid(nforget_ref[d : d + 1, h : h + 1])
                log_weight = gate(0) + ishift_ref[d, h : h + 1, :] + suffix + decay
                largest = jnp.maximum(jnp.max(log_weight, axis=1, keepdims=True), new_input)
                weight = jnp.exp(log_weight - largest)
                weight_out[d, h : h + 1, :] = weight[0:1]
                query = query_ref[d, h : h + 1, :].astype(jnp.float32)
                match = jnp.sum(
                    nkey_ref[d, h : h + 1, :].astype(jnp.float32) * query, axis=1, keepdims=True
                )
                score = jnp.exp(new_input - largest) * match * scaling
                fresh[d, h] = score.astype(jnp.bfloat16).astype(jnp.float32)
                weights[d, h] = weight


    def convolve():
        for d in range(nd):
            ext[:, 0:8, :] = jnp.zeros((hl, 8, dk), jnp.float32)
            for at in range(nsp):
                for c in range(C):
                    if chunks[c][0] == 0:
                        arrived(d, at, c)
                for h in range(hl):
                    ext[h, 8 + at * pos : 8 + (at + 1) * pos, :] = final[
                        d, h, at * pos : (at + 1) * pos, :
                    ].astype(jnp.float32)
                    tap = conv_ref[
                        :, pl.ds(pl.multiple_of((t * hl + h) * dk, dk), dk)
                    ]
                    summed = None
                    for o in range(taps):
                        start = 8 - (taps - 1) + o + at * pos
                        term = ext[h, start : start + pos, :] * tap[o : o + 1, :]
                        summed = term if summed is None else summed + term
                    keys_out[d, h, at * pos : (at + 1) * pos, :] = jax.nn.silu(summed).astype(
                        jnp.bfloat16
                    )
            for h in range(hl):
                query = jnp.broadcast_to(query_ref[d, h : h + 1, :], (8, dk))
                matched = lax.dot_general(
                    query, keys_out[d, h], (((1,), (1,)), ((), ())), preferred_element_type=jnp.float32
                )
                scores[d, h] = (weights[d, h] * matched * scaling).astype(jnp.bfloat16)

    for k in range(n - 1):
        relay_step(k, C)
    for k in range(n - 1):
        for c in range(C):
            if k == n - 2 and c == C - 1:
                if n == 2:
                    weigh()
                convolve()
            relay_step(k, c)
        if k == 0 and n > 2:
            weigh()
    if n == 1:
        weigh()
        convolve()

    for d in range(nd):
        for at in range(nsp):
            for c in range(C):
                if chunks[c][0] == 1:
                    arrived(d, at, c)
        for h in range(hl):
            score = scores[d, h]
            denominator = jnp.sum(score.astype(jnp.float32), axis=1, keepdims=True) + fresh[d, h]
            numerator = jnp.dot(score, values_out[d, h], preferred_element_type=jnp.float32)
            numerator = numerator + fresh[d, h] * nvalue_ref[d, h : h + 1, :].astype(jnp.float32)
            result = numerator / jnp.maximum(jnp.abs(denominator), 1.0)
            read_out[d, h : h + 1, :] = result[0:1].astype(jnp.bfloat16)

    for k in range(n):
        b = t if k == n - 1 else origin(k)
        for i in range(ns):
            for c in range(C + 1):
                if k < n - 1:
                    s1_copy(k, i, c).wait_send()
                forward(k, b, i, c, False)

def write_out(*refs):
    count = (len(refs) - 1) // 2
    sem = refs[-1]
    copies = [
        pltpu.make_async_copy(refs[i], refs[count + i], sem.at[i]) for i in range(count)
    ]
    for copy in copies:
        copy.start()
    for copy in copies:
        copy.wait()


def shards(
    n,
    nsp,
    layer_input,
    norm_gain,
    key_weight,
    value_weight,
    input_gate_weight,
    forget_gate_weight,
    conv_weight,
    input_shift,
    forget_shift,
    new_query,
    new_key,
    new_value,
    new_input,
    new_forget,
):
    ns, pos, width = layer_input.shape
    nd, hl, length = input_shift.shape
    dk = new_query.shape[2]
    heads = input_gate_weight.shape[1]
    taps = conv_weight.shape[0]
    dims = (n, nsp, ns, nd, pos, heads, hl, dk, taps)
    C = 2 * SPLIT
    bf16, f32 = jnp.bfloat16, jnp.float32
    vmem = pl.BlockSpec(memory_space=pltpu.VMEM)
    hbm = pl.BlockSpec(memory_space=pltpu.HBM)
    dma = pltpu.SemaphoreType.DMA
    out_shape=(
        jax.ShapeDtypeStruct((nd, hl, length, dk), bf16),
        jax.ShapeDtypeStruct((nd, hl, length, dk), bf16),
        jax.ShapeDtypeStruct((nd, hl, length), f32),
        jax.ShapeDtypeStruct((nd, hl, dk), bf16),
    )
    held = pl.pallas_call(
        functools.partial(kernel, dims),
        out_shape=tuple(pltpu.VMEM(o.shape, o.dtype) for o in out_shape),
        in_specs=[vmem] * 12 + [hbm] * 2,
        out_specs=(vmem,) * 4,
        scratch_shapes=[
            pltpu.VMEM((n, 2, width, hl * dk), bf16),
            pltpu.VMEM((ns, pos, width), bf16),
            pltpu.VMEM((n, ns, 2, hl, pos, dk), bf16),
            pltpu.VMEM((n, ns, 2, hl, pos, dk), bf16),
            pltpu.VMEM((nd, hl, length, dk), bf16),
            pltpu.VMEM((ns, 2 * heads, pos), bf16),
            pltpu.VMEM((n, ns, 2 * heads, pos), bf16),
            pltpu.VMEM((nd, nsp, 2 * heads, pos), bf16),
            pltpu.VMEM((hl, 8 + length, dk), f32),
            dma((n, 2)),
            dma((n, ns, C + 1)),
            dma((n, ns, C + 1)),
            dma((n, ns, C + 1)),
            dma((nd, nsp, C + 1)),
        ],
        compiler_params=pltpu.CompilerParams(
            collective_id=0, has_side_effects=True, vmem_limit_bytes=60 * 1024 * 1024
        ),
    )(
        layer_input,
        norm_gain,
        input_gate_weight.T,
        forget_gate_weight.T,
        conv_weight,
        input_shift,
        forget_shift,
        new_query,
        new_key,
        new_value,
        new_input,
        new_forget,
        key_weight,
        value_weight,
    )
    return pl.pallas_call(
        write_out,
        out_shape=out_shape,
        in_specs=[vmem] * len(out_shape),
        out_specs=(hbm,) * len(out_shape),
        scratch_shapes=[dma((len(out_shape),))],
        compiler_params=pltpu.CompilerParams(vmem_limit_bytes=8 * 1024 * 1024),
    )(*held)


def solution(mesh):
    in_specs = (
        P(("grp", "tp"), "sp", None),
        P(),
        P(),
        P(),
        P(),
        P(),
        P(),
        P(("grp", "sp"), "tp", None),
        P(("grp", "sp"), "tp", None),
        P(("grp", "sp"), "tp", None),
        P(("grp", "sp"), "tp", None),
        P(("grp", "sp"), "tp", None),
        P(("grp", "sp"), "tp"),
        P(("grp", "sp"), "tp"),
    )
    out_specs = (
        P(("grp", "sp"), "tp", None, None),
        P(("grp", "sp"), "tp", None, None),
        P(("grp", "sp"), "tp", None),
        P(("grp", "sp"), "tp", None),
    )
    body = functools.partial(shards, mesh.shape["tp"], mesh.shape["sp"])
    return jax.shard_map(body, mesh=mesh, in_specs=in_specs, out_specs=out_specs, check_vma=False)
```

profile of v0, /device:TPU:0, one launch (start us, length us, event | category | flops | bytes accessed | tf_op | source)
XLA Modules:
  0.0 41.2 jit_solution(2806875786857468140)
XLA Ops:
  0.6 39.6 %shard_map.165 = (bf16[1,2,1024,128]{3,2,1,0:T(8,128)(2,1)S(1)}, bf16[1,2,1024,128]{3,2,1,0:T(8,128)(2,1)S(1)}, f32[1,2,1024]{2,1,0:T(2,128)S(1)}, bf16[1,2,128]{2,1,0:T(2,128)(2,1)S(1)}) custom-call(bf16[1,256,2048]{2,1,0:T(8,128)(2,1)} %x_ref.1, bf16[2048]{0:T(1024)(128)(2,1)} %gain_ref.1, bf16[8,2048]{1,0:T(8,128)(2,1)} %bitcast.2, ...), custom_call_target="tpu_custom_call" | custom-call | tf_op jit(solution)/shard_map/pallas_call | solution.py:357
  40.2 1.0 %shard_map.166 = (bf16[1,2,1024,128]{3,2,1,0:T(8,128)(2,1)}, bf16[1,2,1024,128]{3,2,1,0:T(8,128)(2,1)}, f32[1,2,1024]{2,1,0:T(2,128)}, bf16[1,2,128]{2,1,0:T(2,128)(2,1)}) custom-call(bf16[1,2,1024,128]{3,2,1,0:T(8,128)(2,1)S(1)} %get-tuple-element.8.refs_0_, bf16[1,2,1024,128]{3,2,1,0:T(8,128)(2,1)S(1)} %get-tuple-element.9.refs_1_, ...), custom_call_target="tpu_custom_call" | custom-call | tf_op jit(solution)/shard_map/pallas_call | solution.py:397
where the time goes:
time: 41.4 us; the launch traced here: 41.2 us
  Pallas kernels  40.6 us (98%)
  between operations  0.64 us (2%)
    pallas_call x1, Pallas kernels, shards(): pl.pallas_call(functools.partial(kernel, dims), out_shape=tuple((pltpu.VM...  39.6 us
    pallas_call x1, Pallas kernels, shards(): pl.pallas_call(write_out, out_shape=out_shape, in_specs=[vmem] * len(out_...  1.01 us

commit v1 on v0

v1 whole, which is shorter than its diff:
```python
import functools

import jax
import jax.numpy as jnp
from jax import lax
from jax.experimental import pallas as pl
from jax.experimental.pallas import tpu as pltpu
from jax.sharding import PartitionSpec as P

MESH = pl.DeviceIdType.MESH
epsilon = 1e-06


def log_sigmoid(x):
    return jnp.minimum(x, 0.0) - jnp.log1p(jnp.exp(-jnp.abs(x)))


def kernel(
    dims,
    x_hbm,
    gain_hbm,
    wi_hbm,
    wf_hbm,
    conv_hbm,
    ishift_hbm,
    fshift_hbm,
    query_hbm,
    nkey_hbm,
    nvalue_hbm,
    ninput_hbm,
    nforget_hbm,
    wk_hbm,
    wv_hbm,
    keys_out,
    values_out,
    weight_out,
    read_out,
    x_ref,
    gain_ref,
    wgate,
    conv_ref,
    ishift_ref,
    fshift_ref,
    query_ref,
    nkey_ref,
    nvalue_ref,
    ninput_ref,
    nforget_ref,
    wbuf,
    scaled,
    normed,
    rs,
    comp,
    gcomp,
    final,
    gfinal,
    ext,
    in_sem,
    w_sem,
    small_sem,
    send_sem,
    f_recv,
):
    n, nsp, ns, nd, pos, heads, hl, dk, taps = dims
    G = 2
    length = nsp * pos
    width = x_ref.shape[2]
    nt = max(1, nd // ns)
    nq = max(1, ns // nd)
    t = lax.axis_index("tp")
    p = lax.axis_index("sp")
    low = 2 * t < n

    first = (p * nd) // ns
    barrier = pltpu.get_barrier_semaphore()
    for m in range(nt):
        for a in range(nsp):
            peer = {"sp": lax.rem(p + a, nsp), "tp": first + m}

            def greet(peer=peer):
                pl.semaphore_signal(barrier, inc=1, device_id=peer, device_id_type=MESH)

            if a:
                greet()
            else:
                pl.when(first + m != t)(greet)
    own = ((t >= first) & (t < first + nt)).astype(jnp.int32)

    def target(k):
        down = jnp.where(k < n - 1 - t, n - 1 - k, n - 2 - k)
        up = jnp.where(k < t, k, k + 1)
        return jnp.where(k == n - 1, t, jnp.where(low, down, up))

    def weight_copy(k, kv):
        columns = pl.ds(pl.multiple_of(target(k) * (hl * dk), dk), hl * dk)
        source = wv_hbm if kv else wk_hbm
        return pltpu.make_async_copy(source.at[:, columns], wbuf.at[k, kv], w_sem.at[k, kv])

    x_copy = pltpu.make_async_copy(x_hbm, x_ref, in_sem.at[0])
    gain_copy = pltpu.make_async_copy(gain_hbm, gain_ref, in_sem.at[1])
    wi_copy = pltpu.make_async_copy(wi_hbm, wgate.at[0:heads], in_sem.at[2])
    wf_copy = pltpu.make_async_copy(wf_hbm, wgate.at[heads : 2 * heads], in_sem.at[3])
    x_copy.start()
    gain_copy.start()
    weight_copy(0, 0).start()
    weight_copy(0, 1).start()
    wi_copy.start()
    wf_copy.start()
    for k in range(1, n):
        for kv in range(2):
            weight_copy(k, kv).start()
    own_columns = pl.ds(pl.multiple_of(t * (hl * dk), dk), hl * dk)
    small = [
        pltpu.make_async_copy(a, b, small_sem.at[at])
        for at, (a, b) in enumerate(
            (
                (conv_hbm.at[:, own_columns], conv_ref),
                (ishift_hbm, ishift_ref),
                (fshift_hbm, fshift_ref),
                (query_hbm, query_ref),
                (nkey_hbm, nkey_ref),
                (nvalue_hbm, nvalue_ref),
                (ninput_hbm, ninput_ref),
                (nforget_hbm, nforget_ref),
            )
        )
    ]
    for copy in small:
        copy.start()

    gain_copy.wait()
    gain = gain_ref[...].astype(jnp.float32).reshape(1, -1)
    x_copy.wait()
    step = 32
    for i in range(ns):
        for at in range(0, pos, step):
            wide = x_ref[i, at : at + step, :].astype(jnp.float32)
            scaled[i, at : at + step, :] = (wide * gain).astype(jnp.bfloat16)
            mean = jnp.mean(wide * wide, axis=-1, keepdims=True)
            rs[i, at : at + step, :] = jnp.broadcast_to(lax.rsqrt(mean + epsilon), (step, dk))

    def s_source(k, i, c):
        return gcomp.at[i] if c == G else comp.at[k, i, c]

    def f_target(d, at, c):
        if c == G:
            return gfinal.at[d, at]
        window = pl.ds(pl.multiple_of(at * pos, pos), pos)
        return (values_out if c else final).at[d, :, window, :]

    def send(k, i, c, begin):
        s = t * ns + i
        q = s // nd
        d = lax.rem(s, nd)
        source = s_source(k, i, c)
        remote = pltpu.make_async_remote_copy(
            src_ref=source,
            dst_ref=f_target(d, p, c),
            send_sem=send_sem.at[k, i, c],
            recv_sem=f_recv.at[d, p, c],
            device_id={"sp": q, "tp": target(k)},
            device_id_type=MESH,
        )
        away = (k < n - 1) | (q != p)

        @pl.when(away)
        def _():
            if begin:
                remote.start()
            else:
                remote.wait_send()

        if begin:

            @pl.when(jnp.logical_not(away))
            def _():
                pltpu.make_async_copy(source, f_target(d, p, c), f_recv.at[d, p, c]).start()

    def gates():
        wi_copy.wait()
        wf_copy.wait()
        for i in range(ns):

            @pl.loop(0, pos // step)
            def _(at):
                window = pl.ds(pl.multiple_of(at * step, step), step)
                wide = x_ref[i, window, :].astype(jnp.float32)
                normed[i, window, :] = (wide * rs[i, window, 0:1] * gain).astype(jnp.bfloat16)

            g = lax.dot_general(
                normed[i], wgate[...], (((1,), (1,)), ((), ())), preferred_element_type=jnp.float32
            )
            gcomp[i] = g.T.astype(jnp.bfloat16)

    @pl.loop(0, n)
    def _(k):
        for kv in range(2):
            weight_copy(k, kv).wait()
            for i in range(ns):
                y = jnp.dot(scaled[i], wbuf[k, kv], preferred_element_type=jnp.float32)
                for h in range(hl):
                    comp[k, i, kv, h] = (y[:, h * dk : (h + 1) * dk] * rs[i]).astype(jnp.bfloat16)
            if kv == 0:

                @pl.when(k == 0)
                def _():
                    pl.semaphore_wait(barrier, nq * n - own)

            for i in range(ns):
                send(k, i, kv, True)

        @pl.when(k == 0)
        def _():
            gates()
            for to in range(n):
                for i in range(ns):
                    send(to, i, G, True)

    def arrived(d, at, c):
        place = f_target(d, at, c)
        pltpu.make_async_copy(place, place, f_recv.at[d, at, c]).wait()

    scaling = dk ** (-0.5)
    lane = lax.broadcasted_iota(jnp.int32, (8, length), 1)
    row = lax.broadcasted_iota(jnp.int32, (2 * heads, pos), 0)
    weights, fresh, scores = {}, {}, {}
    for copy in small:
        copy.wait()

    for d in range(nd):
        for at in range(nsp):
            arrived(d, at, G)
        for h in range(hl):

            def gate(base):
                pieces = [
                    jnp.sum(
                        jnp.where(row == base + t * hl + h, gfinal[d, at].astype(jnp.float32), 0.0),
                        axis=0,
                        keepdims=True,
                    )
                    for at in range(nsp)
                ]
                return jnp.concatenate(pieces, axis=1)

            log_forget = log_sigmoid(gate(heads) + fshift_ref[d, h : h + 1, :])
            suffix = pltpu.roll(jnp.broadcast_to(log_forget, (8, length)), length - 1, 1)
            suffix = jnp.where(lane < length - 1, suffix, 0.0)
            hop = 1
            while hop < length:
                moved = pltpu.roll(suffix, length - hop, 1)
                suffix = suffix + jnp.where(lane < length - hop, moved, 0.0)
                hop *= 2
            new_input = ninput_ref[d : d + 1, h : h + 1]
            decay = log_sigmoid(nforget_ref[d : d + 1, h : h + 1])
            log_weight = gate(0) + ishift_ref[d, h : h + 1, :] + suffix + decay
            largest = jnp.maximum(jnp.max(log_weight, axis=1, keepdims=True), new_input)
            weight = jnp.exp(log_weight - largest)
            weight_out[d, h : h + 1, :] = weight[0:1]
            query = query_ref[d, h : h + 1, :].astype(jnp.float32)
            match = jnp.sum(
                nkey_ref[d, h : h + 1, :].astype(jnp.float32) * query, axis=1, keepdims=True
            )
            score = jnp.exp(new_input - largest) * match * scaling
            fresh[d, h] = score.astype(jnp.bfloat16).astype(jnp.float32)
            weights[d, h] = weight

    for d in range(nd):
        ext[:, 0:8, :] = jnp.zeros((hl, 8, dk), jnp.float32)
        for at in range(nsp):
            arrived(d, at, 0)
            for h in range(hl):
                ext[h, 8 + at * pos : 8 + (at + 1) * pos, :] = final[
                    d, h, at * pos : (at + 1) * pos, :
                ].astype(jnp.float32)
                tap = conv_ref[:, h * dk : (h + 1) * dk]
                summed = None
                for o in range(taps):
                    start = 8 - (taps - 1) + o + at * pos
                    term = ext[h, start : start + pos, :] * tap[o : o + 1, :]
                    summed = term if summed is None else summed + term
                keys_out[d, h, at * pos : (at + 1) * pos, :] = jax.nn.silu(summed).astype(
                    jnp.bfloat16
                )
        for h in range(hl):
            query = jnp.broadcast_to(query_ref[d, h : h + 1, :], (8, dk))
            matched = lax.dot_general(
                query, keys_out[d, h], (((1,), (1,)), ((), ())), preferred_element_type=jnp.float32
            )
            scores[d, h] = (weights[d, h] * matched * scaling).astype(jnp.bfloat16)

    for d in range(nd):
        for at in range(nsp):
            arrived(d, at, 1)
        for h in range(hl):
            score = scores[d, h]
            denominator = jnp.sum(score.astype(jnp.float32), axis=1, keepdims=True) + fresh[d, h]
            numerator = jnp.dot(score, values_out[d, h], preferred_element_type=jnp.float32)
            numerator = numerator + fresh[d, h] * nvalue_ref[d, h : h + 1, :].astype(jnp.float32)
            result = numerator / jnp.maximum(jnp.abs(denominator), 1.0)
            read_out[d, h : h + 1, :] = result[0:1].astype(jnp.bfloat16)

    for k in range(n):
        for i in range(ns):
            for c in range(G + 1):
                send(k, i, c, False)


def write_out(*refs):
    count = (len(refs) - 1) // 2
    sem = refs[-1]
    copies = [
        pltpu.make_async_copy(refs[i], refs[count + i], sem.at[i]) for i in range(count)
    ]
    for copy in copies:
        copy.start()
    for copy in copies:
        copy.wait()


def shards(
    n,
    nsp,
    layer_input,
    norm_gain,
    key_weight,
    value_weight,
    input_gate_weight,
    forget_gate_weight,
    conv_weight,
    input_shift,
    forget_shift,
    new_query,
    new_key,
    new_value,
    new_input,
    new_forget,
):
    ns, pos, width = layer_input.shape
    nd, hl, length = input_shift.shape
    dk = new_query.shape[2]
    heads = input_gate_weight.shape[1]
    taps = conv_weight.shape[0]
    dims = (n, nsp, ns, nd, pos, heads, hl, dk, taps)
    bf16, f32 = jnp.bfloat16, jnp.float32
    vmem = pl.BlockSpec(memory_space=pltpu.VMEM)
    hbm = pl.BlockSpec(memory_space=pltpu.HBM)
    dma = pltpu.SemaphoreType.DMA
    out_shape = (
        jax.ShapeDtypeStruct((nd, hl, length, dk), bf16),
        jax.ShapeDtypeStruct((nd, hl, length, dk), bf16),
        jax.ShapeDtypeStruct((nd, hl, length), f32),
        jax.ShapeDtypeStruct((nd, hl, dk), bf16),
    )
    held = pl.pallas_call(
        functools.partial(kernel, dims),
        out_shape=tuple(pltpu.VMEM(o.shape, o.dtype) for o in out_shape),
        in_specs=[hbm] * 14,
        out_specs=(vmem,) * 4,
        scratch_shapes=[
            pltpu.VMEM((ns, pos, width), bf16),
            pltpu.VMEM((width,), bf16),
            pltpu.VMEM((2 * heads, width), bf16),
            pltpu.VMEM((taps, hl * dk), f32),
            pltpu.VMEM((nd, hl, length), f32),
            pltpu.VMEM((nd, hl, length), f32),
            pltpu.VMEM((nd, hl, dk), bf16),
            pltpu.VMEM((nd, hl, dk), bf16),
            pltpu.VMEM((nd, hl, dk), bf16),
            pltpu.VMEM((nd, hl), f32),
            pltpu.VMEM((nd, hl), f32),
            pltpu.VMEM((n, 2, width, hl * dk), bf16),
            pltpu.VMEM((ns, pos, width), bf16),
            pltpu.VMEM((ns, pos, width), bf16),
            pltpu.VMEM((ns, pos, dk), f32),
            pltpu.VMEM((n, ns, 2, hl, pos, dk), bf16),
            pltpu.VMEM((ns, 2 * heads, pos), bf16),
            pltpu.VMEM((nd, hl, length, dk), bf16),
            pltpu.VMEM((nd, nsp, 2 * heads, pos), bf16),
            pltpu.VMEM((hl, 8 + length, dk), f32),
            dma((4,)),
            dma((n, 2)),
            dma((8,)),
            dma((n, ns, 3)),
            dma((nd, nsp, 3)),
        ],
        compiler_params=pltpu.CompilerParams(
            collective_id=0, has_side_effects=True, vmem_limit_bytes=60 * 1024 * 1024
        ),
    )(
        layer_input,
        norm_gain,
        input_gate_weight.T,
        forget_gate_weight.T,
        conv_weight,
        input_shift,
        forget_shift,
        new_query,
        new_key,
        new_value,
        new_input,
        new_forget,
        key_weight,
        value_weight,
    )
    return pl.pallas_call(
        write_out,
        out_shape=out_shape,
        in_specs=[vmem] * len(out_shape),
        out_specs=(hbm,) * len(out_shape),
        scratch_shapes=[dma((len(out_shape),))],
        compiler_params=pltpu.CompilerParams(vmem_limit_bytes=8 * 1024 * 1024),
    )(*held)


def solution(mesh):
    in_specs = (
        P(("grp", "tp"), "sp", None),
        P(),
        P(),
        P(),
        P(),
        P(),
        P(),
        P(("grp", "sp"), "tp", None),
        P(("grp", "sp"), "tp", None),
        P(("grp", "sp"), "tp", None),
        P(("grp", "sp"), "tp", None),
        P(("grp", "sp"), "tp", None),
        P(("grp", "sp"), "tp"),
        P(("grp", "sp"), "tp"),
    )
    out_specs = (
        P(("grp", "sp"), "tp", None, None),
        P(("grp", "sp"), "tp", None, None),
        P(("grp", "sp"), "tp", None),
        P(("grp", "sp"), "tp", None),
    )
    body = functools.partial(shards, mesh.shape["tp"], mesh.shape["sp"])
    return jax.shard_map(body, mesh=mesh, in_specs=in_specs, out_specs=out_specs, check_vma=False)
```

time: 41.4 us -> 31.8 us (0.77)
  the two profiles are of different devices: /device:TPU:0 before, /device:TPU:12 now
where the time goes in v1:
time: 31.8 us; the launch traced here: 31.7 us
  Pallas kernels  31 us (97%)
  between operations  0.64 us (2%)
    pallas_call x1, Pallas kernels, shards(): pl.pallas_call(functools.partial(kernel, dims), out_shape=tuple((pltpu.VM...  30 us
    pallas_call x1, Pallas kernels, shards(): pl.pallas_call(write_out, out_shape=out_shape, in_specs=[vmem] * len(out_...  1.01 us

profile of v1, /device:TPU:12, one launch (start us, length us, event | category | flops | bytes accessed | tf_op | source)
XLA Modules:
  0.0 31.7 jit_solution(5719360509408651603)
XLA Ops:
  0.6 30.0 %shard_map.165 = (bf16[1,2,1024,128]{3,2,1,0:T(8,128)(2,1)S(1)}, bf16[1,2,1024,128]{3,2,1,0:T(8,128)(2,1)S(1)}, f32[1,2,1024]{2,1,0:T(2,128)S(1)}, bf16[1,2,128]{2,1,0:T(2,128)(2,1)S(1)}) custom-call(bf16[1,256,2048]{2,1,0:T(8,128)(2,1)} %x_hbm.1, bf16[2048]{0:T(1024)(128)(2,1)} %gain_hbm.1, bf16[8,2048]{1,0:T(8,128)(2,1)} %bitcast.2, ...), custom_call_target="tpu_custom_call" | custom-call | tf_op jit(solution)/shard_map/pallas_call | solution.py:355
  30.6 1.0 %shard_map.166 = (bf16[1,2,1024,128]{3,2,1,0:T(8,128)(2,1)}, bf16[1,2,1024,128]{3,2,1,0:T(8,128)(2,1)}, f32[1,2,1024]{2,1,0:T(2,128)}, bf16[1,2,128]{2,1,0:T(2,128)(2,1)}) custom-call(bf16[1,2,1024,128]{3,2,1,0:T(8,128)(2,1)S(1)} %get-tuple-element.8.refs_0_, bf16[1,2,1024,128]{3,2,1,0:T(8,128)(2,1)S(1)} %get-tuple-element.9.refs_1_, ...), custom_call_target="tpu_custom_call" | custom-call | tf_op jit(solution)/shard_map/pallas_call | solution.py:406

commit v2 on v1

v2 whole, which is shorter than its diff:
```python
import functools

import jax
import jax.numpy as jnp
from jax import lax
from jax.experimental import pallas as pl
from jax.experimental.pallas import tpu as pltpu
from jax.sharding import PartitionSpec as P

MESH = pl.DeviceIdType.MESH
epsilon = 1e-06
HALVES = 2


def log_sigmoid(x):
    return jnp.minimum(x, 0.0) - jnp.log1p(jnp.exp(-jnp.abs(x)))


def kernel(
    dims,
    x_hbm,
    gain_hbm,
    wi_hbm,
    wf_hbm,
    conv_hbm,
    ishift_hbm,
    fshift_hbm,
    query_hbm,
    nkey_hbm,
    nvalue_hbm,
    ninput_hbm,
    nforget_hbm,
    wk_hbm,
    wv_hbm,
    keys_out,
    values_out,
    weight_out,
    read_out,
    x_ref,
    gain_ref,
    wgate,
    conv_ref,
    shifts,
    fresh_rows,
    fresh_gates,
    wbuf,
    scaled,
    normed,
    rs,
    comp,
    gcomp,
    final,
    gfinal,
    ext,
    x_sem,
    in_sem,
    w_sem,
    send_sem,
    f_recv,
    ready,
):
    n, nsp, ns, nd, pos, heads, hl, dk, taps = dims
    G = 2
    length = nsp * pos
    width = x_ref.shape[2]
    nt = max(1, nd // ns)
    nq = max(1, ns // nd)
    t = lax.axis_index("tp")
    p = lax.axis_index("sp")
    low = 2 * t < n

    first = (p * nd) // ns
    late = n >= 4
    far = t == n - 1 if late else False
    barrier = pltpu.get_barrier_semaphore()

    def tell(semaphore, sp, tp):
        pl.semaphore_signal(
            semaphore, inc=1, device_id={"sp": sp, "tp": tp}, device_id_type=MESH
        )

    def greet(only_far):
        for m in range(nt):
            for a in range(nsp):
                to = first + m
                wanted = None if a else to != t
                if only_far:
                    wanted = to == n - 1 if a else (to == n - 1) & (to != t)

                def one(a=a, to=to):
                    tell(barrier, lax.rem(p + a, nsp), to)

                one() if wanted is None else pl.when(wanted)(one)

    own = ((t >= first) & (t < first + nt)).astype(jnp.int32)
    if late:

        @pl.when(far)
        def _():
            greet(True)

        @pl.when(jnp.logical_not(far))
        def _():
            for m in range(nq):
                tell(barrier, (t * ns) // nd + m, n - 1)
            greet(False)

        ends = ((first <= n - 1) & (n - 1 < first + nt)).astype(jnp.int32)
        expected = jnp.where(far, nq * n - own + nsp * (nt - ends), nq * (n - 1) - own)
    else:
        greet(False)
        expected = nq * n - own

    def met():
        pl.semaphore_wait(barrier, expected)
        if late:

            @pl.when(far)
            def _():
                for m in range(nt):
                    for a in range(nsp):

                        @pl.when(first + m != n - 1)
                        def _():
                            tell(ready, lax.rem(p + a, nsp), first + m)

    def target(k):
        down = jnp.where(k < n - 1 - t, n - 1 - k, n - 2 - k)
        if late:
            down = jnp.where(k == 0, n - 2, jnp.where(k == 1, n - 1, down))
        up = jnp.where(k < t, k, k + 1)
        return jnp.where(k == n - 1, t, jnp.where(low, down, up))

    def weight_copy(k, kv):
        columns = pl.ds(pl.multiple_of(target(k) * (hl * dk), dk), hl * dk)
        source = wv_hbm if kv else wk_hbm
        slot = kv if isinstance(k, int) and k == 0 else 1 + k
        return pltpu.make_async_copy(source.at[:, columns], wbuf.at[k, kv], w_sem.at[slot])

    half = pos // HALVES
    x_copies = [
        pltpu.make_async_copy(
            x_hbm.at[:, at * half : (at + 1) * half], x_ref.at[:, at * half : (at + 1) * half], x_sem.at[at]
        )
        for at in range(HALVES)
    ]
    own_columns = pl.ds(pl.multiple_of(t * (hl * dk), dk), hl * dk)
    groups = (
        (gain_ref, ((gain_hbm, gain_ref),)),
        (wgate, ((wi_hbm, wgate.at[0:heads]), (wf_hbm, wgate.at[heads : 2 * heads]))),
        (conv_ref, ((conv_hbm.at[:, own_columns], conv_ref),)),
        (shifts, ((ishift_hbm, shifts.at[0]), (fshift_hbm, shifts.at[1]))),
        (
            fresh_rows,
            ((query_hbm, fresh_rows.at[0]), (nkey_hbm, fresh_rows.at[1]), (nvalue_hbm, fresh_rows.at[2])),
        ),
        (fresh_gates, ((ninput_hbm, fresh_gates.at[0]), (nforget_hbm, fresh_gates.at[1]))),
    )

    def load(g):
        for source, place in groups[g][1]:
            pltpu.make_async_copy(source, place, in_sem.at[g]).start()

    def loaded(g):
        whole = groups[g][0]
        pltpu.make_async_copy(whole, whole, in_sem.at[g]).wait()

    load(0)
    x_copies[0].start()
    weight_copy(0, 0).start()
    for copy in x_copies[1:]:
        copy.start()

    def start_rest():
        weight_copy(0, 1).start()
        load(1)
        for k in range(1, n):
            for kv in range(2):
                weight_copy(k, kv).start()
        for g in range(2, len(groups)):
            load(g)

    loaded(0)
    gain = gain_ref[...].astype(jnp.float32).reshape(1, -1)
    step = 32

    def scale(part):
        x_copies[part].wait()
        for i in range(ns):
            for at in range(part * half, (part + 1) * half, step):
                wide = x_ref[i, at : at + step, :].astype(jnp.float32)
                scaled[i, at : at + step, :] = (wide * gain).astype(jnp.bfloat16)
                mean = jnp.mean(wide * wide, axis=-1, keepdims=True)
                rs[i, at : at + step, :] = jnp.broadcast_to(lax.rsqrt(mean + epsilon), (step, dk))

    def send(k, i, c, part=None):
        s = t * ns + i
        q = s // nd
        d = lax.rem(s, nd)
        to = k if c == G else target(k)
        mine = to == t
        if c == G:
            source, place = gcomp.at[k, i], gfinal.at[d, p]
        else:
            rows = half if part is not None else pos
            lead = half * part if part is not None else 0
            source = comp.at[k, i, c, :, pl.ds(lead, rows), :]
            window = pl.ds(pl.multiple_of(p * pos + lead, rows), rows)
            place = (values_out if c else final).at[d, :, window, :]
        slot = jnp.where(mine, 1, 0)
        remote = pltpu.make_async_remote_copy(
            src_ref=source,
            dst_ref=place,
            send_sem=send_sem.at[slot, c // G],
            recv_sem=f_recv.at[d, c],
            device_id={"sp": q, "tp": to},
            device_id_type=MESH,
        )
        away = jnp.logical_not(mine & (q == p))
        pl.when(away)(lambda: remote.start())

        @pl.when(jnp.logical_not(away))
        def _():
            pltpu.make_async_copy(source, place, f_recv.at[d, c]).start()

    def gates():
        loaded(1)
        for i in range(ns):

            @pl.loop(0, pos // step)
            def _(at):
                window = pl.ds(pl.multiple_of(at * step, step), step)
                wide = x_ref[i, window, :].astype(jnp.float32)
                normed[i, window, :] = (wide * rs[i, window, 0:1] * gain).astype(jnp.bfloat16)

            g = lax.dot_general(
                normed[i], wgate[...], (((1,), (1,)), ((), ())), preferred_element_type=jnp.float32
            )
            g = g.T
            for to in range(n):
                lines = [
                    g[base + to * hl + h : base + to * hl + h + 1, at * 128 : (at + 1) * 128]
                    for base in (0, heads)
                    for h in range(hl)
                    for at in range(pos // 128)
                ]
                gcomp[to, i] = jnp.concatenate(lines, axis=0).astype(jnp.bfloat16)

    def project(k, kv, lead, rows):
        for i in range(ns):
            y = jnp.dot(
                scaled[i, lead : lead + rows], wbuf[k, kv], preferred_element_type=jnp.float32
            )
            for h in range(hl):
                comp[k, i, kv, h, lead : lead + rows] = (
                    y[:, h * dk : (h + 1) * dk] * rs[i, lead : lead + rows]
                ).astype(jnp.bfloat16)

    scale(0)
    weight_copy(0, 0).wait()
    start_rest()
    for part in range(HALVES):
        if part:
            scale(part)
        project(0, 0, part * half, half)
        if part == 0:
            met()
        for i in range(ns):
            send(0, i, 0, part)
    weight_copy(0, 1).wait()
    project(0, 1, 0, pos)
    for i in range(ns):
        send(0, i, 1)
    gates()
    if late:

        @pl.when(jnp.logical_not(far))
        def _():
            pl.semaphore_wait(ready, nq)

    for to in range(n):
        for i in range(ns):
            send(to, i, G)

    @pl.loop(1, n)
    def _(k):
        pltpu.make_async_copy(wbuf.at[k], wbuf.at[k], w_sem.at[1 + k]).wait()
        for kv in range(2):
            project(k, kv, 0, pos)
            for i in range(ns):
                send(k, i, kv)

    def arrived(d, c):
        place = (final.at[d], values_out.at[d], gfinal.at[d])[c]
        pltpu.make_async_copy(place, place, f_recv.at[d, c]).wait()

    scaling = dk ** (-0.5)
    lane = lax.broadcasted_iota(jnp.int32, (8, length), 1)
    weights, fresh, scores = {}, {}, {}
    for g in range(2, len(groups)):
        loaded(g)

    for d in range(nd):
        arrived(d, G)
        for h in range(hl):

            def gate(which):
                lead = (which * hl + h) * (pos // 128)
                return jnp.concatenate(
                    [
                        gfinal[d, at].astype(jnp.float32)[lead + q : lead + q + 1]
                        for at in range(nsp)
                        for q in range(pos // 128)
                    ],
                    axis=1,
                )

            log_forget = log_sigmoid(gate(1) + shifts[1, d, h : h + 1, :])
            suffix = pltpu.roll(jnp.broadcast_to(log_forget, (8, length)), length - 1, 1)
            suffix = jnp.where(lane < length - 1, suffix, 0.0)
            hop = 1
            while hop < length:
                moved = pltpu.roll(suffix, length - hop, 1)
                suffix = suffix + jnp.where(lane < length - hop, moved, 0.0)
                hop *= 2
            new_input = fresh_gates[0, d : d + 1, h : h + 1]
            decay = log_sigmoid(fresh_gates[1, d : d + 1, h : h + 1])
            log_weight = gate(0) + shifts[0, d, h : h + 1, :] + suffix + decay
            largest = jnp.maximum(jnp.max(log_weight, axis=1, keepdims=True), new_input)
            weight = jnp.exp(log_weight - largest)
            weight_out[d, h : h + 1, :] = weight[0:1]
            query = fresh_rows[0, d, h : h + 1, :].astype(jnp.float32)
            match = jnp.sum(
                fresh_rows[1, d, h : h + 1, :].astype(jnp.float32) * query, axis=1, keepdims=True
            )
            score = jnp.exp(new_input - largest) * match * scaling
            fresh[d, h] = score.astype(jnp.bfloat16).astype(jnp.float32)
            weights[d, h] = weight

    for d in range(nd):
        ext[:, 0:8, :] = jnp.zeros((hl, 8, dk), jnp.float32)
        arrived(d, 0)
        for at in range(nsp):
            for h in range(hl):
                ext[h, 8 + at * pos : 8 + (at + 1) * pos, :] = final[
                    d, h, at * pos : (at + 1) * pos, :
                ].astype(jnp.float32)
                tap = conv_ref[:, h * dk : (h + 1) * dk]
                summed = None
                for o in range(taps):
                    start = 8 - (taps - 1) + o + at * pos
                    term = ext[h, start : start + pos, :] * tap[o : o + 1, :]
                    summed = term if summed is None else summed + term
                keys_out[d, h, at * pos : (at + 1) * pos, :] = jax.nn.silu(summed).astype(
                    jnp.bfloat16
                )
        for h in range(hl):
            query = jnp.broadcast_to(fresh_rows[0, d, h : h + 1, :], (8, dk))
            matched = lax.dot_general(
                query, keys_out[d, h], (((1,), (1,)), ((), ())), preferred_element_type=jnp.float32
            )
            scores[d, h] = (weights[d, h] * matched * scaling).astype(jnp.bfloat16)

    for d in range(nd):
        arrived(d, 1)
        for h in range(hl):
            score = scores[d, h]
            denominator = jnp.sum(score.astype(jnp.float32), axis=1, keepdims=True) + fresh[d, h]
            numerator = jnp.dot(score, values_out[d, h], preferred_element_type=jnp.float32)
            numerator = numerator + fresh[d, h] * fresh_rows[2, d, h : h + 1, :].astype(jnp.float32)
            result = numerator / jnp.maximum(jnp.abs(denominator), 1.0)
            read_out[d, h : h + 1, :] = result[0:1].astype(jnp.bfloat16)

    def sent(place, slot, c):
        pltpu.make_async_copy(place, place, send_sem.at[slot, c]).wait()

    if n > 1:
        sent(comp.at[0 : n - 1], 0, 0)
        sent(gcomp.at[0 : n - 1], 0, 1)
    kept = sum(((t * ns + i) // nd == p).astype(jnp.int32) for i in range(ns))
    for count in range(ns):

        @pl.when(kept == count)
        def _():
            sent(comp.at[n - 1, 0 : ns - count], 1, 0)
            sent(gcomp.at[n - 1, 0 : ns - count], 1, 1)


def write_out(*refs):
    count = (len(refs) - 1) // 2
    sem = refs[-1]
    copies = [
        pltpu.make_async_copy(refs[i], refs[count + i], sem.at[i]) for i in range(count)
    ]
    for copy in copies:
        copy.start()
    for copy in copies:
        copy.wait()


def shards(
    n,
    nsp,
    layer_input,
    norm_gain,
    key_weight,
    value_weight,
    input_gate_weight,
    forget_gate_weight,
    conv_weight,
    input_shift,
    forget_shift,
    new_query,
    new_key,
    new_value,
    new_input,
    new_forget,
):
    ns, pos, width = layer_input.shape
    nd, hl, length = input_shift.shape
    dk = new_query.shape[2]
    heads = input_gate_weight.shape[1]
    taps = conv_weight.shape[0]
    dims = (n, nsp, ns, nd, pos, heads, hl, dk, taps)
    bf16, f32 = jnp.bfloat16, jnp.float32
    vmem = pl.BlockSpec(memory_space=pltpu.VMEM)
    hbm = pl.BlockSpec(memory_space=pltpu.HBM)
    dma = pltpu.SemaphoreType.DMA
    out_shape = (
        jax.ShapeDtypeStruct((nd, hl, length, dk), bf16),
        jax.ShapeDtypeStruct((nd, hl, length, dk), bf16),
        jax.ShapeDtypeStruct((nd, hl, length), f32),
        jax.ShapeDtypeStruct((nd, hl, dk), bf16),
    )
    held = pl.pallas_call(
        functools.partial(kernel, dims),
        out_shape=tuple(pltpu.VMEM(o.shape, o.dtype) for o in out_shape),
        in_specs=[hbm] * 14,
        out_specs=(vmem,) * 4,
        scratch_shapes=[
            pltpu.VMEM((ns, pos, width), bf16),
            pltpu.VMEM((width,), bf16),
            pltpu.VMEM((2 * heads, width), bf16),
            pltpu.VMEM((taps, hl * dk), f32),
            pltpu.VMEM((2, nd, hl, length), f32),
            pltpu.VMEM((3, nd, hl, dk), bf16),
            pltpu.VMEM((2, nd, hl), f32),
            pltpu.VMEM((n, 2, width, hl * dk), bf16),
            pltpu.VMEM((ns, pos, width), bf16),
            pltpu.VMEM((ns, pos, width), bf16),
            pltpu.VMEM((ns, pos, dk), f32),
            pltpu.VMEM((n, ns, 2, hl, pos, dk), bf16),
            pltpu.VMEM((n, ns, 2 * hl * pos // 128, 128), bf16),
            pltpu.VMEM((nd, hl, length, dk), bf16),
            pltpu.VMEM((nd, nsp, 2 * hl * pos // 128, 128), bf16),
            pltpu.VMEM((hl, 8 + length, dk), f32),
            dma((HALVES,)),
            dma((6,)),
            dma((n + 1,)),
            dma((2, 2)),
            dma((nd, 3)),
            pltpu.SemaphoreType.REGULAR,
        ],
        compiler_params=pltpu.CompilerParams(
            collective_id=0, has_side_effects=True, vmem_limit_bytes=60 * 1024 * 1024
        ),
    )(
        layer_input,
        norm_gain,
        input_gate_weight.T,
        forget_gate_weight.T,
        conv_weight,
        input_shift,
        forget_shift,
        new_query,
        new_key,
        new_value,
        new_input,
        new_forget,
        key_weight,
        value_weight,
    )
    return pl.pallas_call(
        write_out,
        out_shape=out_shape,
        in_specs=[vmem] * len(out_shape),
        out_specs=(hbm,) * len(out_shape),
        scratch_shapes=[dma((len(out_shape),))],
        compiler_params=pltpu.CompilerParams(vmem_limit_bytes=8 * 1024 * 1024),
    )(*held)


def solution(mesh):
    in_specs = (
        P(("grp", "tp"), "sp", None),
        P(),
        P(),
        P(),
        P(),
        P(),
        P(),
        P(("grp", "sp"), "tp", None),
        P(("grp", "sp"), "tp", None),
        P(("grp", "sp"), "tp", None),
        P(("grp", "sp"), "tp", None),
        P(("grp", "sp"), "tp", None),
        P(("grp", "sp"), "tp"),
        P(("grp", "sp"), "tp"),
    )
    out_specs = (
        P(("grp", "sp"), "tp", None, None),
        P(("grp", "sp"), "tp", None, None),
        P(("grp", "sp"), "tp", None),
        P(("grp", "sp"), "tp", None),
    )
    body = functools.partial(shards, mesh.shape["tp"], mesh.shape["sp"])
    return jax.shard_map(body, mesh=mesh, in_specs=in_specs, out_specs=out_specs, check_vma=False)
```

time: 31.8 us -> 29 us (0.912)
  Pallas kernels: 31 us -> 28.3 us
    pallas_call x1, Pallas kernels: 30 us -> 27.2 us  [shards(): pl.pallas_call(functools.partial(kernel, dims), out_shape=tuple((pltpu.VM...]
where the time goes in v2:
time: 29 us; the launch traced here: 28.9 us
  Pallas kernels  28.3 us (98%)
  between operations  0.64 us (2%)
    pallas_call x1, Pallas kernels, shards(): pl.pallas_call(functools.partial(kernel, dims), out_shape=tuple((pltpu.VM...  27.2 us
    pallas_call x1, Pallas kernels, shards(): pl.pallas_call(write_out, out_shape=out_shape, in_specs=[vmem] * len(out_...  1.01 us

profile of v2, /device:TPU:12, one launch (start us, length us, event | category | flops | bytes accessed | tf_op | source)
XLA Modules:
  0.0 28.9 jit_solution(15868769014314937518)
XLA Ops:
  0.6 27.2 %shard_map.165 = (bf16[1,2,1024,128]{3,2,1,0:T(8,128)(2,1)S(1)}, bf16[1,2,1024,128]{3,2,1,0:T(8,128)(2,1)S(1)}, f32[1,2,1024]{2,1,0:T(2,128)S(1)}, bf16[1,2,128]{2,1,0:T(2,128)(2,1)S(1)}) custom-call(bf16[1,256,2048]{2,1,0:T(8,128)(2,1)} %x_hbm.1, bf16[2048]{0:T(1024)(128)(2,1)} %gain_hbm.1, bf16[8,2048]{1,0:T(8,128)(2,1)} %bitcast.2, ...), custom_call_target="tpu_custom_call" | custom-call | tf_op jit(solution)/shard_map/pallas_call | solution.py:435
  27.9 1.0 %shard_map.166 = (bf16[1,2,1024,128]{3,2,1,0:T(8,128)(2,1)}, bf16[1,2,1024,128]{3,2,1,0:T(8,128)(2,1)}, f32[1,2,1024]{2,1,0:T(2,128)}, bf16[1,2,128]{2,1,0:T(2,128)(2,1)}) custom-call(bf16[1,2,1024,128]{3,2,1,0:T(8,128)(2,1)S(1)} %get-tuple-element.8.refs_0_, bf16[1,2,1024,128]{3,2,1,0:T(8,128)(2,1)S(1)} %get-tuple-element.9.refs_1_, ...), custom_call_target="tpu_custom_call" | custom-call | tf_op jit(solution)/shard_map/pallas_call | solution.py:483

commit v3 on v2

--- a/solution.py
+++ b/solution.py
@@ -9,7 +9,7 @@
 
 MESH = pl.DeviceIdType.MESH
 epsilon = 1e-06
-HALVES = 2
+EARLY = 2
 
 
 def log_sigmoid(x):
@@ -35,7 +35,9 @@
     keys_out,
     values_out,
     weight_out,
-    read_out,
+    score_out,
+    base_out,
+    floor_out,
     x_ref,
     gain_ref,
     wgate,
@@ -52,9 +54,7 @@
     final,
     gfinal,
     ext,
-    x_sem,
-    in_sem,
-    w_sem,
+    load_sem,
     send_sem,
     f_recv,
     ready,
@@ -111,18 +111,13 @@
         greet(False)
         expected = nq * n - own
 
-    def met():
-        pl.semaphore_wait(barrier, expected)
-        if late:
-
-            @pl.when(far)
-            def _():
-                for m in range(nt):
-                    for a in range(nsp):
-
-                        @pl.when(first + m != n - 1)
-                        def _():
-                            tell(ready, lax.rem(p + a, nsp), first + m)
+    def answer():
+        for m in range(nt):
+            for a in range(nsp):
+
+                @pl.when(first + m != n - 1)
+                def _():
+                    tell(ready, lax.rem(p + a, nsp), first + m)
 
     def target(k):
         down = jnp.where(k < n - 1 - t, n - 1 - k, n - 2 - k)
@@ -131,22 +126,32 @@
         up = jnp.where(k < t, k, k + 1)
         return jnp.where(k == n - 1, t, jnp.where(low, down, up))
 
-    def weight_copy(k, kv):
-        columns = pl.ds(pl.multiple_of(target(k) * (hl * dk), dk), hl * dk)
+    def weight_copy(k, kv, head=0, count=hl, slot=2):
+        columns = pl.ds(pl.multiple_of((target(k) * hl + head) * dk, dk), count * dk)
         source = wv_hbm if kv else wk_hbm
-        slot = kv if isinstance(k, int) and k == 0 else 1 + k
-        return pltpu.make_async_copy(source.at[:, columns], wbuf.at[k, kv], w_sem.at[slot])
-
-    half = pos // HALVES
+        place = wbuf.at[k, kv, :, head * dk : (head + count) * dk]
+        return pltpu.make_async_copy(source.at[:, columns], place, load_sem.at[slot])
+
+    early = pos // EARLY
+    spans = ((0, early), (early, pos - early))
     x_copies = [
         pltpu.make_async_copy(
-            x_hbm.at[:, at * half : (at + 1) * half], x_ref.at[:, at * half : (at + 1) * half], x_sem.at[at]
+            x_hbm.at[:, lead : lead + rows], x_ref.at[:, lead : lead + rows], load_sem.at[at]
         )
-        for at in range(HALVES)
+        for at, (lead, rows) in enumerate(spans)
     ]
+    gain_copy = pltpu.make_async_copy(gain_hbm, gain_ref, load_sem.at[2])
+    key_first = weight_copy(0, 0, 0, 1, 3)
+    key_rest = weight_copy(0, 0, 1, hl - 1, 4) if hl > 1 else None
+    value_first = weight_copy(0, 1, 0, hl, 5)
+    gain_copy.start()
+    x_copies[0].start()
+    key_first.start()
+    x_copies[1].start()
+    if key_rest is not None:
+        key_rest.start()
     own_columns = pl.ds(pl.multiple_of(t * (hl * dk), dk), hl * dk)
     groups = (
-        (gain_ref, ((gain_hbm, gain_ref),)),
         (wgate, ((wi_hbm, wgate.at[0:heads]), (wf_hbm, wgate.at[heads : 2 * heads]))),
         (conv_ref, ((conv_hbm.at[:, own_columns], conv_ref),)),
         (shifts, ((ishift_hbm, shifts.at[0]), (fshift_hbm, shifts.at[1]))),
@@ -157,61 +162,52 @@
         (fresh_gates, ((ninput_hbm, fresh_gates.at[0]), (nforget_hbm, fresh_gates.at[1]))),
     )
 
+    slots = (0, 1, 3, 4, 5)
+
     def load(g):
         for source, place in groups[g][1]:
-            pltpu.make_async_copy(source, place, in_sem.at[g]).start()
+            pltpu.make_async_copy(source, place, load_sem.at[slots[g]]).start()
 
     def loaded(g):
         whole = groups[g][0]
-        pltpu.make_async_copy(whole, whole, in_sem.at[g]).wait()
-
-    load(0)
-    x_copies[0].start()
-    weight_copy(0, 0).start()
-    for copy in x_copies[1:]:
-        copy.start()
+        pltpu.make_async_copy(whole, whole, load_sem.at[slots[g]]).wait()
 
     def start_rest():
-        weight_copy(0, 1).start()
-        load(1)
         for k in range(1, n):
             for kv in range(2):
                 weight_copy(k, kv).start()
-        for g in range(2, len(groups)):
+        for g in range(1, len(groups)):
             load(g)
 
-    loaded(0)
+    gain_copy.wait()
     gain = gain_ref[...].astype(jnp.float32).reshape(1, -1)
     step = 32
 
     def scale(part):
         x_copies[part].wait()
         for i in range(ns):
-            for at in range(part * half, (part + 1) * half, step):
+            for at in range(spans[part][0], sum(spans[part]), step):
                 wide = x_ref[i, at : at + step, :].astype(jnp.float32)
                 scaled[i, at : at + step, :] = (wide * gain).astype(jnp.bfloat16)
                 mean = jnp.mean(wide * wide, axis=-1, keepdims=True)
                 rs[i, at : at + step, :] = jnp.broadcast_to(lax.rsqrt(mean + epsilon), (step, dk))
 
-    def send(k, i, c, part=None):
+    def send(k, i, c, lead=0, rows=pos, head=0, count=hl):
         s = t * ns + i
         q = s // nd
         d = lax.rem(s, nd)
         to = k if c == G else target(k)
         mine = to == t
         if c == G:
-            source, place = gcomp.at[k, i], gfinal.at[d, p]
+            source, place = gcomp.at[k * ns + i], gfinal.at[d, p]
         else:
-            rows = half if part is not None else pos
-            lead = half * part if part is not None else 0
-            source = comp.at[k, i, c, :, pl.ds(lead, rows), :]
-            window = pl.ds(pl.multiple_of(p * pos + lead, rows), rows)
-            place = (values_out if c else final).at[d, :, window, :]
-        slot = jnp.where(mine, 1, 0)
+            source = comp.at[k * ns + i, c, head : head + count, lead : lead + rows, :]
+            window = pl.ds(pl.multiple_of(p * pos + lead, rows & -rows), rows)
+            place = (values_out if c else final).at[d, head : head + count, window, :]
         remote = pltpu.make_async_remote_copy(
             src_ref=source,
             dst_ref=place,
-            send_sem=send_sem.at[slot, c // G],
+            send_sem=send_sem.at[c // G],
             recv_sem=f_recv.at[d, c],
             device_id={"sp": q, "tp": to},
             device_id_type=MESH,
@@ -224,7 +220,7 @@
             pltpu.make_async_copy(source, place, f_recv.at[d, c]).start()
 
     def gates():
-        loaded(1)
+        loaded(0)
         for i in range(ns):
 
             @pl.loop(0, pos // step)
@@ -244,33 +240,42 @@
                     for h in range(hl)
                     for at in range(pos // 128)
                 ]
-                gcomp[to, i] = jnp.concatenate(lines, axis=0).astype(jnp.bfloat16)
-
-    def project(k, kv, lead, rows):
+                gcomp[to * ns + i] = jnp.concatenate(lines, axis=0).astype(jnp.bfloat16)
+
+    def project(k, kv, lead=0, rows=pos, head=0, count=hl):
         for i in range(ns):
             y = jnp.dot(
-                scaled[i, lead : lead + rows], wbuf[k, kv], preferred_element_type=jnp.float32
+                scaled[i, lead : lead + rows],
+                wbuf[k, kv, :, head * dk : (head + count) * dk],
+                preferred_element_type=jnp.float32,
             )
-            for h in range(hl):
-                comp[k, i, kv, h, lead : lead + rows] = (
+            for h in range(count):
+                comp[k * ns + i, kv, head + h, lead : lead + rows] = (
                     y[:, h * dk : (h + 1) * dk] * rs[i, lead : lead + rows]
                 ).astype(jnp.bfloat16)
 
+    def emit(k, kv, *piece):
+        project(k, kv, *piece)
+        if piece == (0, early, 0, 1):
+            pl.semaphore_wait(barrier, expected)
+        for i in range(ns):
+            send(k, i, kv, *piece)
+
     scale(0)
-    weight_copy(0, 0).wait()
+    key_first.wait()
+    value_first.start()
+    load(0)
+    emit(0, 0, 0, early, 0, 1)
+    scale(1)
+    emit(0, 0, early, pos - early, 0, 1)
+    if late:
+        pl.when(far)(answer)
+    if key_rest is not None:
+        key_rest.wait()
+        emit(0, 0, 0, pos, 1, hl - 1)
+    value_first.wait()
     start_rest()
-    for part in range(HALVES):
-        if part:
-            scale(part)
-        project(0, 0, part * half, half)
-        if part == 0:
-            met()
-        for i in range(ns):
-            send(0, i, 0, part)
-    weight_copy(0, 1).wait()
-    project(0, 1, 0, pos)
-    for i in range(ns):
-        send(0, i, 1)
+    emit(0, 1)
     gates()
     if late:
 
@@ -282,13 +287,13 @@
         for i in range(ns):
             send(to, i, G)
 
+    if n > 1:
+        pltpu.make_async_copy(wbuf.at[1:n], wbuf.at[1:n], load_sem.at[2]).wait()
+
     @pl.loop(1, n)
     def _(k):
-        pltpu.make_async_copy(wbuf.at[k], wbuf.at[k], w_sem.at[1 + k]).wait()
         for kv in range(2):
-            project(k, kv, 0, pos)
-            for i in range(ns):
-                send(k, i, kv)
+            emit(k, kv)
 
     def arrived(d, c):
         place = (final.at[d], values_out.at[d], gfinal.at[d])[c]
@@ -296,8 +301,8 @@
 
     scaling = dk ** (-0.5)
     lane = lax.broadcasted_iota(jnp.int32, (8, length), 1)
-    weights, fresh, scores = {}, {}, {}
-    for g in range(2, len(groups)):
+    weights, fresh = {}, {}
+    for g in range(1, len(groups)):
         loaded(g)
 
     for d in range(nd):
@@ -359,41 +364,38 @@
             matched = lax.dot_general(
                 query, keys_out[d, h], (((1,), (1,)), ((), ())), preferred_element_type=jnp.float32
             )
-            scores[d, h] = (weights[d, h] * matched * scaling).astype(jnp.bfloat16)
+            score = (weights[d, h] * matched * scaling).astype(jnp.bfloat16)
+            score_out[d, h] = score
+            denominator = jnp.sum(score.astype(jnp.float32), axis=1, keepdims=True) + fresh[d, h]
+            floor_out[d, h] = jnp.broadcast_to(jnp.maximum(jnp.abs(denominator), 1.0), (8, dk))
+            base = fresh[d, h] * fresh_rows[2, d, h : h + 1, :].astype(jnp.float32)
+            base_out[d, h] = jnp.broadcast_to(base, (8, dk))
 
     for d in range(nd):
         arrived(d, 1)
-        for h in range(hl):
-            score = scores[d, h]
-            denominator = jnp.sum(score.astype(jnp.float32), axis=1, keepdims=True) + fresh[d, h]
-            numerator = jnp.dot(score, values_out[d, h], preferred_element_type=jnp.float32)
-            numerator = numerator + fresh[d, h] * fresh_rows[2, d, h : h + 1, :].astype(jnp.float32)
-            result = numerator / jnp.maximum(jnp.abs(denominator), 1.0)
-            read_out[d, h : h + 1, :] = result[0:1].astype(jnp.bfloat16)
-
-    def sent(place, slot, c):
-        pltpu.make_async_copy(place, place, send_sem.at[slot, c]).wait()
-
-    if n > 1:
-        sent(comp.at[0 : n - 1], 0, 0)
-        sent(gcomp.at[0 : n - 1], 0, 1)
+
     kept = sum(((t * ns + i) // nd == p).astype(jnp.int32) for i in range(ns))
-    for count in range(ns):
+    for count in range(ns + 1):
 
         @pl.when(kept == count)
         def _():
-            sent(comp.at[n - 1, 0 : ns - count], 1, 0)
-            sent(gcomp.at[n - 1, 0 : ns - count], 1, 1)
-
-
-def write_out(*refs):
-    count = (len(refs) - 1) // 2
-    sem = refs[-1]
-    copies = [
-        pltpu.make_async_copy(refs[i], refs[count + i], sem.at[i]) for i in range(count)
-    ]
-    for copy in copies:
+            for c, buffer in enumerate((comp, gcomp)):
+                place = buffer.at[0 : n * ns - count]
+                pltpu.make_async_copy(place, place, send_sem.at[c]).wait()
+
+
+def write_out(keys, values, weight, score, base, floor, keys_hbm, values_hbm, weight_hbm, read_hbm, read, sem):
+    pairs = ((values, values_hbm), (keys, keys_hbm), (weight, weight_hbm), (read, read_hbm))
+    copies = [pltpu.make_async_copy(*pair, sem.at[at]) for at, pair in enumerate(pairs)]
+    for copy in copies[:3]:
         copy.start()
+    nd, hl = values.shape[:2]
+    for d in range(nd):
+        for h in range(hl):
+            numerator = jnp.dot(score[d, h], values[d, h], preferred_element_type=jnp.float32)
+            result = (numerator + base[d, h]) / floor[d, h]
+            read[d, h : h + 1, :] = result[0:1].astype(jnp.bfloat16)
+    copies[3].start()
     for copy in copies:
         copy.wait()
 
@@ -432,11 +434,16 @@
         jax.ShapeDtypeStruct((nd, hl, length), f32),
         jax.ShapeDtypeStruct((nd, hl, dk), bf16),
     )
+    held_shape = out_shape[:3] + (
+        jax.ShapeDtypeStruct((nd, hl, 8, length), bf16),
+        jax.ShapeDtypeStruct((nd, hl, 8, dk), f32),
+        jax.ShapeDtypeStruct((nd, hl, 8, dk), f32),
+    )
     held = pl.pallas_call(
         functools.partial(kernel, dims),
-        out_shape=tuple(pltpu.VMEM(o.shape, o.dtype) for o in out_shape),
+        out_shape=tuple(pltpu.VMEM(o.shape, o.dtype) for o in held_shape),
         in_specs=[hbm] * 14,
-        out_specs=(vmem,) * 4,
+        out_specs=(vmem,) * 6,
         scratch_shapes=[
             pltpu.VMEM((ns, pos, width), bf16),
             pltpu.VMEM((width,), bf16),
@@ -449,15 +456,13 @@
             pltpu.VMEM((ns, pos, width), bf16),
             pltpu.VMEM((ns, pos, width), bf16),
             pltpu.VMEM((ns, pos, dk), f32),
-            pltpu.VMEM((n, ns, 2, hl, pos, dk), bf16),
-            pltpu.VMEM((n, ns, 2 * hl * pos // 128, 128), bf16),
+            pltpu.VMEM((n * ns, 2, hl, pos, dk), bf16),
+            pltpu.VMEM((n * ns, 2 * hl * pos // 128, 128), bf16),
             pltpu.VMEM((nd, hl, length, dk), bf16),
             pltpu.VMEM((nd, nsp, 2 * hl * pos // 128, 128), bf16),
             pltpu.VMEM((hl, 8 + length, dk), f32),
-            dma((HALVES,)),
             dma((6,)),
-            dma((n + 1,)),
-            dma((2, 2)),
+            dma((2,)),
             dma((nd, 3)),
             pltpu.SemaphoreType.REGULAR,
         ],
@@ -483,9 +488,9 @@
     return pl.pallas_call(
         write_out,
         out_shape=out_shape,
-        in_specs=[vmem] * len(out_shape),
+        in_specs=[vmem] * len(held_shape),
         out_specs=(hbm,) * len(out_shape),
-        scratch_shapes=[dma((len(out_shape),))],
+        scratch_shapes=[pltpu.VMEM((nd, hl, dk), bf16), dma((len(out_shape),))],
         compiler_params=pltpu.CompilerParams(vmem_limit_bytes=8 * 1024 * 1024),
     )(*held)
 

time: 29 us -> 28.7 us (0.990)
  Pallas kernels: 28.3 us -> 27.9 us
    pallas_call x1, Pallas kernels: 27.2 us -> 26.8 us  [shards(): pl.pallas_call(functools.partial(kernel, dims), out_shape=tuple((pltpu.VM...]
where the time goes in v3:
time: 28.7 us; the launch traced here: 28.5 us
  Pallas kernels  27.9 us (97%)
  between operations  0.64 us (2%)
    pallas_call x1, Pallas kernels, shards(): pl.pallas_call(functools.partial(kernel, dims), out_shape=tuple((pltpu.VM...  26.8 us
    pallas_call x1, Pallas kernels, shards(): pl.pallas_call(write_out, out_shape=out_shape, in_specs=[vmem] * len(held...  1.01 us

profile of v3, /device:TPU:12, one launch (start us, length us, event | category | flops | bytes accessed | tf_op | source)
XLA Modules:
  0.0 28.5 jit_solution(12015623043187068255)
XLA Ops:
  0.6 26.8 %shard_map.165 = (bf16[1,2,1024,128]{3,2,1,0:T(8,128)(2,1)S(1)}, bf16[1,2,1024,128]{3,2,1,0:T(8,128)(2,1)S(1)}, f32[1,2,1024]{2,1,0:T(2,128)S(1)}, bf16[1,2,8,10...) custom-call(bf16[1,256,2048]{2,1,0:T(8,128)(2,1)} %x_hbm.1, ...), custom_call_target="tpu_custom_call" | custom-call | tf_op jit(solution)/shard_map/pallas_call | solution.py:442
  27.5 1.0 %shard_map.166 = (bf16[1,2,1024,128]{3,2,1,0:T(8,128)(2,1)}, bf16[1,2,1024,128]{3,2,1,0:T(8,128)(2,1)}, f32[1,2,1024]{2,1,0:T(2,128)}, bf16[1,2,128]{2,1,0:T(2,128)(2,1)}) custom-call(bf16[1,2,1024,128]{3,2,1,0:T(8,128)(2,1)S(1)} %get-tuple-element.10.keys, bf16[1,2,1024,128]{3,2,1,0:T(8,128)(2,1)S(1)} %get-tuple-element.11.values, ...), custom_call_target="tpu_custom_call" | custom-call | tf_op jit(solution)/shard_map/pallas_call | solution.py:488

commit v4 on v3

--- a/solution.py
+++ b/solution.py
@@ -79,16 +79,22 @@
             semaphore, inc=1, device_id={"sp": sp, "tp": tp}, device_id_type=MESH
         )
 
+    pair = 2 - nsp % 2
+    lead = (p // pair) * pair
+    peers = [lax.rem(lead + a, nsp) for a in range(pair, nsp)]
+    peers += [lead + lax.rem(p + a, pair) for a in range(pair - 1, -1, -1)]
+
     def greet(only_far):
         for m in range(nt):
-            for a in range(nsp):
+            for at, peer in enumerate(peers):
+                a = nsp - 1 - at
                 to = first + m
                 wanted = None if a else to != t
                 if only_far:
                     wanted = to == n - 1 if a else (to == n - 1) & (to != t)
 
-                def one(a=a, to=to):
-                    tell(barrier, lax.rem(p + a, nsp), to)
+                def one(peer=peer, to=to):
+                    tell(barrier, peer, to)
 
                 one() if wanted is None else pl.when(wanted)(one)
 
@@ -101,9 +107,9 @@
 
         @pl.when(jnp.logical_not(far))
         def _():
+            greet(False)
             for m in range(nq):
                 tell(barrier, (t * ns) // nd + m, n - 1)
-            greet(False)
 
         ends = ((first <= n - 1) & (n - 1 < first + nt)).astype(jnp.int32)
         expected = jnp.where(far, nq * n - own + nsp * (nt - ends), nq * (n - 1) - own)
@@ -183,12 +189,15 @@
     gain = gain_ref[...].astype(jnp.float32).reshape(1, -1)
     step = 32
 
+    wide_gain = jnp.broadcast_to(gain, (16, width)).astype(jnp.bfloat16)
+
     def scale(part):
-        x_copies[part].wait()
+        lead, rows = spans[part]
         for i in range(ns):
-            for at in range(spans[part][0], sum(spans[part]), step):
+            for at in range(lead, lead + rows, 16):
+                scaled[i, at : at + 16, :] = x_ref[i, at : at + 16, :] * wide_gain
+            for at in range(lead, lead + rows, step):
                 wide = x_ref[i, at : at + step, :].astype(jnp.float32)
-                scaled[i, at : at + step, :] = (wide * gain).astype(jnp.bfloat16)
                 mean = jnp.mean(wide * wide, axis=-1, keepdims=True)
                 rs[i, at : at + step, :] = jnp.broadcast_to(lax.rsqrt(mean + epsilon), (step, dk))
 
@@ -243,16 +252,19 @@
                 gcomp[to * ns + i] = jnp.concatenate(lines, axis=0).astype(jnp.bfloat16)
 
     def project(k, kv, lead=0, rows=pos, head=0, count=hl):
+        opening = isinstance(k, int) and k == 0
+        rounded = scaled if opening else normed
         for i in range(ns):
             y = jnp.dot(
-                scaled[i, lead : lead + rows],
+                rounded[i, lead : lead + rows],
                 wbuf[k, kv, :, head * dk : (head + count) * dk],
                 preferred_element_type=jnp.float32,
             )
             for h in range(count):
-                comp[k * ns + i, kv, head + h, lead : lead + rows] = (
-                    y[:, h * dk : (h + 1) * dk] * rs[i, lead : lead + rows]
-                ).astype(jnp.bfloat16)
+                block = y[:, h * dk : (h + 1) * dk]
+                if opening:
+                    block = block * rs[i, lead : lead + rows]
+                comp[k * ns + i, kv, head + h, lead : lead + rows] = block.astype(jnp.bfloat16)
 
     def emit(k, kv, *piece):
         project(k, kv, *piece)
@@ -261,11 +273,13 @@
         for i in range(ns):
             send(k, i, kv, *piece)
 
-    scale(0)
+    x_copies[0].wait()
     key_first.wait()
     value_first.start()
     load(0)
+    scale(0)
     emit(0, 0, 0, early, 0, 1)
+    x_copies[1].wait()
     scale(1)
     emit(0, 0, early, pos - early, 0, 1)
     if late:
@@ -371,9 +385,6 @@
             base = fresh[d, h] * fresh_rows[2, d, h : h + 1, :].astype(jnp.float32)
             base_out[d, h] = jnp.broadcast_to(base, (8, dk))
 
-    for d in range(nd):
-        arrived(d, 1)
-
     kept = sum(((t * ns + i) // nd == p).astype(jnp.int32) for i in range(ns))
     for count in range(ns + 1):
 
@@ -382,6 +393,9 @@
             for c, buffer in enumerate((comp, gcomp)):
                 place = buffer.at[0 : n * ns - count]
                 pltpu.make_async_copy(place, place, send_sem.at[c]).wait()
+
+    for d in range(nd):
+        arrived(d, 1)
 
 
 def write_out(keys, values, weight, score, base, floor, keys_hbm, values_hbm, weight_hbm, read_hbm, read, sem):

time: 28.7 us -> 28.7 us (level)
  no operation moved by 1% of the time
where the time goes in v4:
time: 28.7 us; the launch traced here: 28.5 us
  Pallas kernels  27.9 us (97%)
  between operations  0.64 us (2%)
    pallas_call x1, Pallas kernels, shards(): pl.pallas_call(functools.partial(kernel, dims), out_shape=tuple((pltpu.VM...  26.8 us
    pallas_call x1, Pallas kernels, shards(): pl.pallas_call(write_out, out_shape=out_shape, in_specs=[vmem] * len(held...  1.01 us

profile of v4, /device:TPU:12, one launch (start us, length us, event | category | flops | bytes accessed | tf_op | source)
XLA Modules:
  0.0 28.5 jit_solution(9809617724903459843)
XLA Ops:
  0.6 26.8 %shard_map.165 = (bf16[1,2,1024,128]{3,2,1,0:T(8,128)(2,1)S(1)}, bf16[1,2,1024,128]{3,2,1,0:T(8,128)(2,1)S(1)}, f32[1,2,1024]{2,1,0:T(2,128)S(1)}, bf16[1,2,8,10...) custom-call(bf16[1,256,2048]{2,1,0:T(8,128)(2,1)} %x_hbm.1, ...), custom_call_target="tpu_custom_call" | custom-call | tf_op jit(solution)/shard_map/pallas_call | solution.py:456
  27.5 1.0 %shard_map.166 = (bf16[1,2,1024,128]{3,2,1,0:T(8,128)(2,1)}, bf16[1,2,1024,128]{3,2,1,0:T(8,128)(2,1)}, f32[1,2,1024]{2,1,0:T(2,128)}, bf16[1,2,128]{2,1,0:T(2,128)(2,1)}) custom-call(bf16[1,2,1024,128]{3,2,1,0:T(8,128)(2,1)S(1)} %get-tuple-element.10.keys, bf16[1,2,1024,128]{3,2,1,0:T(8,128)(2,1)S(1)} %get-tuple-element.11.values, ...), custom_call_target="tpu_custom_call" | custom-call | tf_op jit(solution)/shard_map/pallas_call | solution.py:502

commit v5 on v4

--- a/solution.py
+++ b/solution.py
@@ -275,10 +275,10 @@
 
     x_copies[0].wait()
     key_first.wait()
+    scale(0)
+    emit(0, 0, 0, early, 0, 1)
     value_first.start()
     load(0)
-    scale(0)
-    emit(0, 0, 0, early, 0, 1)
     x_copies[1].wait()
     scale(1)
     emit(0, 0, early, pos - early, 0, 1)

time: 28.7 us -> 28.7 us (level)
  no operation moved by 1% of the time
where the time goes in v5:
time: 28.7 us; the launch traced here: 28.5 us
  Pallas kernels  27.8 us (97%)
  between operations  0.64 us (2%)
    pallas_call x1, Pallas kernels, shards(): pl.pallas_call(functools.partial(kernel, dims), out_shape=tuple((pltpu.VM...  26.8 us
    pallas_call x1, Pallas kernels, shards(): pl.pallas_call(write_out, out_shape=out_shape, in_specs=[vmem] * len(held...  1.01 us

profile of v5, /device:TPU:12, one launch (start us, length us, event | category | flops | bytes accessed | tf_op | source)
XLA Modules:
  0.0 28.5 jit_solution(9499397348022350387)
XLA Ops:
  0.6 26.8 %shard_map.165 = (bf16[1,2,1024,128]{3,2,1,0:T(8,128)(2,1)S(1)}, bf16[1,2,1024,128]{3,2,1,0:T(8,128)(2,1)S(1)}, f32[1,2,1024]{2,1,0:T(2,128)S(1)}, bf16[1,2,8,10...) custom-call(bf16[1,256,2048]{2,1,0:T(8,128)(2,1)} %x_hbm.1, ...), custom_call_target="tpu_custom_call" | custom-call | tf_op jit(solution)/shard_map/pallas_call | solution.py:456
  27.5 1.0 %shard_map.166 = (bf16[1,2,1024,128]{3,2,1,0:T(8,128)(2,1)}, bf16[1,2,1024,128]{3,2,1,0:T(8,128)(2,1)}, f32[1,2,1024]{2,1,0:T(2,128)}, bf16[1,2,128]{2,1,0:T(2,128)(2,1)}) custom-call(bf16[1,2,1024,128]{3,2,1,0:T(8,128)(2,1)S(1)} %get-tuple-element.10.keys, bf16[1,2,1024,128]{3,2,1,0:T(8,128)(2,1)S(1)} %get-tuple-element.11.values, ...), custom_call_target="tpu_custom_call" | custom-call | tf_op jit(solution)/shard_map/pallas_call | solution.py:502

commit v6 on v5

--- a/solution.py
+++ b/solution.py
@@ -399,7 +399,7 @@
 
 
 def write_out(keys, values, weight, score, base, floor, keys_hbm, values_hbm, weight_hbm, read_hbm, read, sem):
-    pairs = ((values, values_hbm), (keys, keys_hbm), (weight, weight_hbm), (read, read_hbm))
+    pairs = ((weight, weight_hbm), (keys, keys_hbm), (values, values_hbm), (read, read_hbm))
     copies = [pltpu.make_async_copy(*pair, sem.at[at]) for at, pair in enumerate(pairs)]
     for copy in copies[:3]:
         copy.start()

time: 28.7 us -> 28.7 us (level)
  no operation moved by 1% of the time
where the time goes in v6:
time: 28.7 us; the launch traced here: 28.5 us
  Pallas kernels  27.8 us (97%)
  between operations  0.64 us (2%)
    pallas_call x1, Pallas kernels, shards(): pl.pallas_call(functools.partial(kernel, dims), out_shape=tuple((pltpu.VM...  26.8 us
    pallas_call x1, Pallas kernels, shards(): pl.pallas_call(write_out, out_shape=out_shape, in_specs=[vmem] * len(held...  1.01 us

profile of v6, /device:TPU:12, one launch (start us, length us, event | category | flops | bytes accessed | tf_op | source)
XLA Modules:
  0.0 28.5 jit_solution(6587016509395613567)
XLA Ops:
  0.6 26.8 %shard_map.165 = (bf16[1,2,1024,128]{3,2,1,0:T(8,128)(2,1)S(1)}, bf16[1,2,1024,128]{3,2,1,0:T(8,128)(2,1)S(1)}, f32[1,2,1024]{2,1,0:T(2,128)S(1)}, bf16[1,2,8,10...) custom-call(bf16[1,256,2048]{2,1,0:T(8,128)(2,1)} %x_hbm.1, ...), custom_call_target="tpu_custom_call" | custom-call | tf_op jit(solution)/shard_map/pallas_call | solution.py:456
  27.5 1.0 %shard_map.166 = (bf16[1,2,1024,128]{3,2,1,0:T(8,128)(2,1)}, bf16[1,2,1024,128]{3,2,1,0:T(8,128)(2,1)}, f32[1,2,1024]{2,1,0:T(2,128)}, bf16[1,2,128]{2,1,0:T(2,128)(2,1)}) custom-call(bf16[1,2,1024,128]{3,2,1,0:T(8,128)(2,1)S(1)} %get-tuple-element.10.keys, bf16[1,2,1024,128]{3,2,1,0:T(8,128)(2,1)S(1)} %get-tuple-element.11.values, ...), custom_call_target="tpu_custom_call" | custom-call | tf_op jit(solution)/shard_map/pallas_call | solution.py:502
